TPU v7x, 256 devices: a 4x2x16 block of a 4x16x16 slice. The times are simulated.
256 devices in a mesh: grp: 2 (over y), sp: 32 (over z, core), tp: 4 (over x).
Axes of the slice: x: 4, y: 2, z: 16, core: 2. Of those that a mesh axis runs over, the one named last changes fastest.
The devices are a block of a 4x16x16 slice.
Arguments:
- gate_in: bfloat16 [32768, 1536], P(('grp', 'sp'), 'tp'), parts along dimension 0, may hold values from -6 to 6
- mult_in: bfloat16 [32768, 1536], P(('grp', 'sp'), 'tp'), parts along dimension 0, may hold values from -6 to 6
- value_in: bfloat16 [32768, 1536], P(('grp', 'sp'), 'tp'), parts along dimension 0, may hold values from -6 to 6
- doc_ids: int32 [32768], P(('grp', 'sp')), parts along dimension 0, may hold values from 0 to 15, never falling along the last dimension, each value on 1 to 1536 neighbouring positions
- conv_taps: bfloat16 [3, 1536], P(None, 'tp'), may hold values from -3 to 3
- out_proj: bfloat16 [1536, 2048], P('tp'), may hold values from -0.15625 to 0.15625
- resid: bfloat16 [32768, 2048], P(('grp', 'sp', 'tp')), parts along dimension 0, may hold values from -6 to 6
- norm1_gain: float32 [2048], replicated, may hold values from 0.1 to 1.9
- norm1_bias: float32 [2048], replicated, may hold values from -1.5 to 1.5
- expert_ids: int32 [32768, 2], P(('grp', 'sp', 'tp')), parts along dimension 0, may hold values from 0 to 31, all different within a row; in each aligned block of 128 rows (0 to 127, 128 to 255, ...) at most 10 rows name the same one
- expert_wts: float32 [32768, 2], P(('grp', 'sp', 'tp')), parts along dimension 0, may hold values from 0.1 to 1
- w_gate: bfloat16 [32, 2048, 3072], P('sp', None, 'tp'), may hold values from -0.125 to 0.125
- w_up: bfloat16 [32, 2048, 3072], P('sp', None, 'tp'), may hold values from -0.125 to 0.125
- w_down: bfloat16 [32, 3072, 2048], P('sp', 'tp'), may hold values from -0.21582031 to 0.21582031
- norm2_gain: float32 [2048], replicated, may hold values from 0.1 to 1.9
- norm2_bias: float32 [2048], replicated, may hold values from -1.5 to 1.5
Outputs:
- result: bfloat16 [32768, 2048], P(('grp', 'sp', 'tp')), parts along dimension 0
There are 2 independent parts, one for each index of `grp`. A program takes and returns all parts, laid end to end along the dimension named above; an argument that names none is the same for every part. Nothing has to cross between parts.
Inputs may be any that keep to these rules, and one draw needn't show every extreme that they name: `doc_ids`: never falling along the sequence; each document has 1 to 1536 positions and one has exactly 1536. `expert_ids`: each row names 2 different experts. Among the rows of one device no expert is named more than 10 times, and in some device's rows some expert is named exactly 10 times.
All inputs are finite; a program needn't handle non-finite values.
Results may differ from a plain program's by a relative error of at most 0.0095.
Values may be sent and summed in bfloat16 or wider, within the bound.
No kernel may reach another device: no remote copies, remote signals or barrier semaphores. Data moves between devices by JAX's collectives and lax.ppermute only.
A program may use at most 128 MiB of HBM per device.

v0:
```python
import jax
import jax.numpy as jnp
from jax import lax
from jax.sharding import Mesh
from jax.sharding import PartitionSpec as P

SP = ("sp_0", "sp_1")
GRP_SP = ("grp", "sp_0", "sp_1")
GRP_SP_TP = ("grp", "sp_0", "sp_1", "tp")
SUBLANES = 8
residual_scale = 2.0**0.5
norm_eps = 1e-05


def next_in_sequence(x):
    length = lax.axis_size(SP)
    return lax.ppermute(x, SP, [(i, i + 1) for i in range(length - 1)])


def swapped(x):
    return lax.ppermute(x, "sp_1", [(0, 1), (1, 0)])


def layer_norm(pre, gain, bias):
    center = pre - jnp.mean(pre, axis=-1, keepdims=True)
    spread = jnp.mean(center * center, axis=-1, keepdims=True)
    return center * lax.rsqrt(spread + norm_eps) * gain + bias


def dot(a, b):
    return jnp.dot(a, b, preferred_element_type=jnp.float32)


def chunk_slots(capacity, cores):
    width = SUBLANES // cores
    rest = capacity % width
    sizes = ([rest] if rest else []) + [width] * (capacity // width)
    starts = [sum(sizes[:i]) for i in range(len(sizes))]
    return list(zip(starts, sizes))


def shards(
    gate_in,
    mult_in,
    value_in,
    doc_ids,
    conv_taps,
    out_proj,
    resid,
    norm1_gain,
    norm1_bias,
    expert_ids,
    expert_wts,
    w_gate,
    w_up,
    w_down,
    norm2_gain,
    norm2_bias,
):
    n_tp = lax.axis_size("tp")
    chips = lax.axis_size("sp_0")
    cores = lax.axis_size("sp_1")
    experts = chips * cores
    tok_count, top_count = expert_ids.shape
    width = out_proj.shape[1]
    capacity = 5 * tok_count * top_count // (4 * experts)
    tap_weights = conv_taps.astype(jnp.float32)
    taps = tap_weights.shape[0]
    product = mult_in.astype(jnp.float32) * value_in.astype(jnp.float32)
    docs = doc_ids.astype(jnp.float32)
    row_count, channels = product.shape
    tail_docs = jnp.broadcast_to(docs[row_count - taps + 1 :, None], (taps - 1, channels))
    prev = next_in_sequence(jnp.concatenate([product[row_count - taps + 1 :], tail_docs], axis=0))
    prev_rows, prev_docs = (prev[: taps - 1], prev[taps - 1 :, 0])
    meta = jnp.concatenate([expert_ids.astype(jnp.float32).T, expert_wts.T], axis=0)
    metas = jnp.stack([meta, swapped(meta)])
    ext_rows = jnp.concatenate([prev_rows, product], axis=0)
    ext_docs = jnp.concatenate([prev_docs, docs], axis=0)
    filtered = jnp.zeros_like(product)
    for tap_index in range(taps):
        shifted = ext_rows[tap_index : tap_index + row_count]
        same_doc = (ext_docs[tap_index : tap_index + row_count] == docs)[:, None]
        filtered = filtered + tap_weights[tap_index] * jnp.where(same_doc, shifted, 0.0)
    mixed_heads = (gate_in.astype(jnp.float32) * filtered).astype(jnp.bfloat16)
    partial = dot(mixed_heads, out_proj).astype(jnp.bfloat16)
    partials = lax.all_to_all(
        partial.reshape(n_tp, row_count // n_tp, width), "tp", 0, 0, tiled=True
    )
    mixed = jnp.sum(partials.astype(jnp.float32), axis=0)
    hidden_one = layer_norm(
        residual_scale * resid.astype(jnp.float32) + mixed, norm1_gain, norm1_bias
    ).astype(jnp.bfloat16)
    hidden_both = jnp.concatenate([hidden_one, swapped(hidden_one)], axis=0)
    ids, wts = (metas[:, :top_count], metas[:, top_count:])
    numbers = (jnp.arange(chips) * cores + lax.axis_index("sp_1")).astype(jnp.float32)
    named = ids[:, :, None, :] == numbers[None, None, :, None]
    chosen = jnp.any(named, axis=1)
    weight = jnp.sum(jnp.where(named, wts[:, :, None, :], 0.0), axis=1)
    before = (jnp.arange(tok_count)[:, None] < jnp.arange(tok_count)[None, :]).astype(jnp.bfloat16)
    earlier = dot(chosen.astype(jnp.bfloat16), before)
    slot_of = jnp.where(chosen, earlier, -1.0)

    def selected(start, size, values):
        slots = (start + jnp.arange(size)).astype(jnp.float32)
        hit = slot_of.transpose(1, 0, 2)[:, :, None, None, :] == slots[None, None, :, None, None]
        same = jnp.arange(cores)[:, None] == jnp.arange(cores)[None, :]
        hit = hit & same[None, :, None, :, None]
        picked = jnp.where(hit, values.transpose(1, 0, 2)[:, :, None, None, :], 0.0)
        return picked.reshape(chips * cores * size, cores * tok_count)

    chunks = chunk_slots(capacity, cores)
    ones = jnp.ones_like(weight)
    packed = [
        dot(selected(start, size, ones).astype(jnp.bfloat16), hidden_both)
        .astype(jnp.bfloat16)
        .reshape(chips, cores * size, width)
        for start, size in chunks
    ]
    gathered = []
    for i in range(len(chunks)):
        moved = lax.all_to_all(packed[i], "sp_0", 0, 0, tiled=True)
        rest = tuple(packed[i + 1 :])
        moved, rest = lax.optimization_barrier((moved, rest))
        packed[i + 1 :] = list(rest)
        gathered.append(lax.all_gather(moved.reshape(-1, width), "tp", axis=0, tiled=True))
    scattered = []
    for rows_in in gathered:
        gate_act = dot(rows_in, w_gate[0])
        up_act = dot(rows_in, w_up[0])
        hid = (jax.nn.silu(gate_act) * up_act).astype(jnp.bfloat16)
        piece = dot(hid, w_down[0]).astype(jnp.bfloat16)
        scattered.append(lax.psum_scatter(piece, "tp", scatter_dimension=0, tiled=True))
    total = jnp.zeros((cores * tok_count, width), jnp.float32)
    for i, (start, size) in enumerate(chunks):
        ready = scattered[i].reshape(chips, cores * size, width)
        back = lax.all_to_all(ready, "sp_0", 0, 0, tiled=True).reshape(-1, width)
        factor = selected(start, size, weight)
        high = factor.astype(jnp.bfloat16)
        low = (factor - high.astype(jnp.float32)).astype(jnp.bfloat16)
        total = total + dot(high.T, back) + dot(low.T, back)
    moe = total[:tok_count] + swapped(total[tok_count:])
    return layer_norm(
        residual_scale * hidden_one.astype(jnp.float32) + moe, norm2_gain, norm2_bias
    ).astype(jnp.bfloat16)


def solution(mesh):
    torus = Mesh(
        mesh.devices.reshape(mesh.shape["grp"], -1, 2, mesh.shape["tp"]),
        ("grp", "sp_0", "sp_1", "tp"),
    )
    in_specs = (
        P(GRP_SP, "tp"),
        P(GRP_SP, "tp"),
        P(GRP_SP, "tp"),
        P(GRP_SP),
        P(None, "tp"),
        P("tp", None),
        P(GRP_SP_TP, None),
        P(),
        P(),
        P(GRP_SP_TP, None),
        P(GRP_SP_TP, None),
        P(SP, None, "tp"),
        P(SP, None, "tp"),
        P(SP, "tp", None),
        P(),
        P(),
    )
    out_specs = P(GRP_SP_TP, None)
    return jax.shard_map(
        shards, mesh=torus, in_specs=in_specs, out_specs=out_specs, check_vma=False
    )
```

profile of v0, /device:TPU:33, one launch (start us, length us, event | category | flops | bytes accessed | tf_op | source)
XLA Modules:
  0.0 383.8 jit_solution(6780999300419874182)
XLA Ops:
  8.9 5.7 %collective-permute-start = (f32[4,384]{1,0:T(4,128)S(1)}, f32[4,384]{1,0:T(4,128)S(1)}, u32[]{:S(2)}, u32[]{:S(2)}) collective-permute-start(f32[4,384]{1,0:T(4,128)S(1)} %pad_maximum_fusion.5), channel_id=1, source_target_pairs={{0,4},{4,8},{8,12},{12,16},{16,20},{20,24},{24,28},{28,32},{32,36}... | collective-permute-start | bytes 18440 | tf_op jit(solution)/shard_map/ppermute | solution.py:17
  15.3 15.9 %collective-permute-done = f32[4,384]{1,0:T(4,128)S(1)} collective-permute-done((f32[4,384]{1,0:T(4,128)S(1)}, f32[4,384]{1,0:T(4,128)S(1)}, u32[]{:S(2)}, u32[]{:S(2)}) %collective-permute-start) | collective-permute-done | bytes 6176 | tf_op jit(solution)/shard_map/ppermute | solution.py:17
  32.2 4.4 %convolution_convert_fusion = bf16[512,2048]{1,0:T(8,128)(2,1)} fusion(bf16[384,2048]{1,0:T(8,128)(2,1)} %param.21, f32[2,384]{1,0:T(2,128)S(1)} %slice.63, f32[512,384]{1,0:T(8,128)S(1)} %convert_multiply_fusion, bf16[512,384]{1,0:T(8,128)(2,1)} %param.16, f32[384]{0:T(512)S(1)} %get-tuple-element.16, f32[384]{0:T(512)S(1)} %get-tuple-element.17, ...), kind=kOutput, calls=%fused_computation.21 | convolution fusion | flops 808910848 | bytes 4858880 | tf_op jit(solution)/shard_map/dot_general | solution.py:31
  36.6 4.7 %all-to-all-start = ((bf16[4,128,2048]{2,1,0:T(8,128)(2,1)}), bf16[4,128,2048]{2,1,0:T(8,128)(2,1)}, u32[]{:S(2)}, u32[]{:S(2)}) async-start(bf16[4,128,2048]{2,1,0:T(8,128)(2,1)} %bitcast.127), calls=%async_computation | async-start | bytes 4194304 | tf_op jit(solution)/shard_map/all_to_all | solution.py:86
  42.8 24.7 %all-to-all-done = bf16[4,128,2048]{2,1,0:T(8,128)(2,1)} async-done(((bf16[4,128,2048]{2,1,0:T(8,128)(2,1)}), bf16[4,128,2048]{2,1,0:T(8,128)(2,1)}, u32[]{:S(2)}, u32[]{:S(2)}) %all-to-all-start) | async-done | bytes 2097184 | tf_op jit(solution)/shard_map/all_to_all | solution.py:86
  75.3 6.6 %all-to-all-start.1 = ((bf16[16,4,2048]{2,1,0:T(4,128)(2,1)}), bf16[16,4,2048]{2,1,0:T(4,128)(2,1)S(1)}, u32[]{:S(2)}, u32[]{:S(2)}) async-start(bf16[16,4,2048]{2,1,0:T(4,128)(2,1)} %reshape.246), calls=%async_computation.1 | async-start | bytes 524288 | tf_op jit(solution)/shard_map/all_to_all | solution.py:121
  87.3 8.4 %all-to-all-done.1 = bf16[16,4,2048]{2,1,0:T(4,128)(2,1)S(1)} async-done(((bf16[16,4,2048]{2,1,0:T(4,128)(2,1)}), bf16[16,4,2048]{2,1,0:T(4,128)(2,1)S(1)}, u32[]{:S(2)}, u32[]{:S(2)}) %all-to-all-start.1) | async-done | bytes 262176 | tf_op jit(solution)/shard_map/all_to_all | solution.py:121
  95.7 10.4 %all-to-all-start.3 = ((bf16[16,8,2048]{2,1,0:T(8,128)(2,1)}), bf16[16,8,2048]{2,1,0:T(8,128)(2,1)}, u32[]{:S(2)}, u32[]{:S(2)}) async-start(bf16[16,8,2048]{2,1,0:T(8,128)(2,1)} %fusion.31), calls=%async_computation.4 | async-start | bytes 1048576 | tf_op jit(solution)/shard_map/all_to_all | solution.py:121
  107.1 21.9 %all-to-all-done.3 = bf16[16,8,2048]{2,1,0:T(8,128)(2,1)} async-done(((bf16[16,8,2048]{2,1,0:T(8,128)(2,1)}), bf16[16,8,2048]{2,1,0:T(8,128)(2,1)}, u32[]{:S(2)}, u32[]{:S(2)}) %all-to-all-start.3) | async-done | bytes 524320 | tf_op jit(solution)/shard_map/all_to_all | solution.py:121
  129.1 35.6 %all_to_all.35 = bf16[16,8,2048]{2,1,0:T(8,128)(2,1)} all-to-all(bf16[16,8,2048]{2,1,0:T(8,128)(2,1)} %fusion.32), channel_id=1, replica_groups=mesh['grp'=2,'sp_0'=16,'sp_1'=2,'tp'=4] {'sp_0'}, dimensions={0} | all-to-all | bytes 1048576 | tf_op jit(solution)/shard_map/all_to_all | solution.py:121
  164.9 4.1 %fusion.16 = f32[256,768]{1,0:T(8,128)} fusion(bf16[256,2048]{1,0:T(8,128)(2,1)} %all-gather.4.cloned.1.call-done, bf16[1,2048,768]{2,1,0:T(8,128)(2,1)} %param.27), kind=kOutput, calls=%fused_computation.17 | convolution fusion | flops 805306368 | bytes 4980736 | tf_op jit(solution)/shard_map/dot_general | solution.py:31
  169.0 5.6 %fusion.28 = bf16[256,2048]{1,0:T(8,128)(2,1)} fusion(bf16[1,768,2048]{2,1,0:T(8,128)(2,1)S(1)} %copy-done, bf16[256,2048]{1,0:T(8,128)(2,1)} %all-gather.4.cloned.1.call-done, bf16[1,2048,768]{2,1,0:T(8,128)(2,1)} %param.28, f32[256,768]{1,0:T(8,128)} %fusion.16), kind=kOutput, calls=%fused_computation.27 | convolution fusion | flops 1612316672 | bytes 9175040 | tf_op jit(solution)/shard_map/dot_general | solution.py:31
  177.9 5.5 %fusion.14 = f32[512,768]{1,0:T(8,128)} fusion(bf16[512,2048]{1,0:T(8,128)(2,1)} %all-gather.6.cloned.1.call-done, bf16[1,2048,768]{2,1,0:T(8,128)(2,1)} %param.27), kind=kOutput, calls=%fused_computation.15 | convolution fusion | flops 1610612736 | bytes 6815744 | tf_op jit(solution)/shard_map/dot_general | solution.py:31
  183.3 8.2 %fusion.18 = bf16[512,2048]{1,0:T(8,128)(2,1)} fusion(bf16[1,768,2048]{2,1,0:T(8,128)(2,1)S(1)} %copy-done, f32[512,768]{1,0:T(8,128)} %fusion.14, bf16[512,2048]{1,0:T(8,128)(2,1)} %all-gather.6.cloned.1.call-done, bf16[1,2048,768]{2,1,0:T(8,128)(2,1)} %param.28), kind=kOutput, calls=%fused_computation.19 | convolution fusion | flops 3224633344 | bytes 12058624 | tf_op jit(solution)/shard_map/dot_general | solution.py:31
  191.7 24.9 %all-gather.8.cloned.1.call-done = bf16[512,2048]{1,0:T(8,128)(2,1)} async-done(((bf16[128,2048]{1,0:T(8,128)(2,1)}), bf16[512,2048]{1,0:T(8,128)(2,1)}) %all-gather.8.cloned.1.call-update) | async-done | bytes 2097168 | tf_op jit(solution)/shard_map/all_gather | solution.py:125
  216.7 5.5 %fusion.12 = f32[512,768]{1,0:T(8,128)} fusion(bf16[512,2048]{1,0:T(8,128)(2,1)} %all-gather.8.cloned.1.call-done, bf16[1,2048,768]{2,1,0:T(8,128)(2,1)} %param.27), kind=kOutput, calls=%fused_computation.13 | convolution fusion | flops 1610612736 | bytes 6815744 | tf_op jit(solution)/shard_map/dot_general | solution.py:31
  222.1 8.3 %fusion.21 = bf16[512,2048]{1,0:T(8,128)(2,1)} fusion(bf16[1,768,2048]{2,1,0:T(8,128)(2,1)S(1)} %copy-done, f32[512,768]{1,0:T(8,128)} %fusion.12, bf16[512,2048]{1,0:T(8,128)(2,1)} %all-gather.8.cloned.1.call-done, bf16[1,2048,768]{2,1,0:T(8,128)(2,1)} %param.28), kind=kOutput, calls=%fused_computation.20 | convolution fusion | flops 3224633344 | bytes 12058624 | tf_op jit(solution)/shard_map/dot_general | solution.py:31
  230.5 17.2 %reduce-scatter.4.cloned.1.call-done = bf16[64,2048]{1,0:T(8,128)(2,1)} async-done(((bf16[256,2048]{1,0:T(8,128)(2,1)}), bf16[64,2048]{1,0:T(8,128)(2,1)}) %reduce-scatter.4.cloned.1.call-update) | async-done | bytes 262160 | tf_op jit(solution)/shard_map/reduce_scatter | solution.py:132
  248.7 24.5 %all_to_all.36 = bf16[16,4,2048]{2,1,0:T(4,128)(2,1)} all-to-all(bf16[16,4,2048]{2,1,0:T(4,128)(2,1)S(1)} %reshape.250), channel_id=1, replica_groups=mesh['grp'=2,'sp_0'=16,'sp_1'=2,'tp'=4] {'sp_0'}, dimensions={0} | all-to-all | bytes 524288 | tf_op jit(solution)/shard_map/all_to_all | solution.py:136
  273.3 13.8 %reduce-scatter.6.cloned.1.call-done = bf16[128,2048]{1,0:T(8,128)(2,1)} async-done(((bf16[512,2048]{1,0:T(8,128)(2,1)}), bf16[128,2048]{1,0:T(8,128)(2,1)}) %reduce-scatter.6.cloned.1.call-update) | async-done | bytes 524304 | tf_op jit(solution)/shard_map/reduce_scatter | solution.py:132
  287.0 35.0 %all_to_all.37 = bf16[16,8,2048]{2,1,0:T(8,128)(2,1)} all-to-all(bf16[16,8,2048]{2,1,0:T(8,128)(2,1)} %bitcast.130), channel_id=1, replica_groups=mesh['grp'=2,'sp_0'=16,'sp_1'=2,'tp'=4] {'sp_0'}, dimensions={0} | all-to-all | bytes 1048576 | tf_op jit(solution)/shard_map/all_to_all | solution.py:136
  325.0 12.1 %all-to-all-start.6 = ((bf16[16,8,2048]{2,1,0:T(8,128)(2,1)}), bf16[16,8,2048]{2,1,0:T(8,128)(2,1)}, u32[]{:S(2)}, u32[]{:S(2)}) async-start(bf16[16,8,2048]{2,1,0:T(8,128)(2,1)} %bitcast.129), calls=%async_computation.9 | async-start | bytes 1048576 | tf_op jit(solution)/shard_map/all_to_all | solution.py:136
  345.1 14.9 %all-to-all-done.6 = bf16[16,8,2048]{2,1,0:T(8,128)(2,1)} async-done(((bf16[16,8,2048]{2,1,0:T(8,128)(2,1)}), bf16[16,8,2048]{2,1,0:T(8,128)(2,1)}, u32[]{:S(2)}, u32[]{:S(2)}) %all-to-all-start.6) | async-done | bytes 524320 | tf_op jit(solution)/shard_map/all_to_all | solution.py:136
  365.8 7.2 %collective-permute-start.3 = (f32[128,2048]{1,0:T(8,128)S(1)}, f32[128,2048]{1,0:T(8,128)S(1)}, u32[]{:S(2)}, u32[]{:S(2)}) collective-permute-start(f32[128,2048]{1,0:T(8,128)S(1)} %slice.71), channel_id=1, source_target_pairs={{0,4},{4,0},{1,5},{5,1},{2,6},{6,2},{3,7},{7,3},{8,12},{12,8},{9,1... | collective-permute-start | bytes 3145736 | tf_op jit(solution)/shard_map/ppermute | solution.py:21
  (120 shorter events, 44.8 us)
Async XLA Ops:
  6.5 162.5 %copy-start = (bf16[1,768,2048]{2,1,0:T(8,128)(2,1)S(1)}, bf16[1,768,2048]{2,1,0:T(8,128)(2,1)}, u32[]{:S(2)}) copy-start(bf16[1,768,2048]{2,1,0:T(8,128)(2,1)} %param.29) | copy-start | bytes 9437188
  8.9 22.4 %collective-permute-start = (f32[4,384]{1,0:T(4,128)S(1)}, f32[4,384]{1,0:T(4,128)S(1)}, u32[]{:S(2)}, u32[]{:S(2)}) collective-permute-start(f32[4,384]{1,0:T(4,128)S(1)} %pad_maximum_fusion.5), channel_id=1, source_target_pairs={{0,4},{4,8},{8,12},{12,16},{16,20},{20,24},{24,28},{28,32},{32,36}... | collective-permute-start | bytes 18440 | tf_op jit(solution)/shard_map/ppermute | solution.py:17
  36.6 4.7 %copy-start.19 = (s32[128,2]{0,1:T(2,128)S(1)}, s32[128,2]{0,1:T(2,128)}, u32[]{:S(2)}) copy-start(s32[128,2]{0,1:T(2,128)} %param.25) | copy-start | bytes 3076
  36.6 4.7 %copy-start.20 = (f32[128,2]{0,1:T(2,128)S(1)}, f32[128,2]{0,1:T(2,128)}, u32[]{:S(2)}) copy-start(f32[128,2]{0,1:T(2,128)} %param.26) | copy-start | bytes 3076
  36.6 30.9 %all-to-all-start = ((bf16[4,128,2048]{2,1,0:T(8,128)(2,1)}), bf16[4,128,2048]{2,1,0:T(8,128)(2,1)}, u32[]{:S(2)}, u32[]{:S(2)}) async-start(bf16[4,128,2048]{2,1,0:T(8,128)(2,1)} %bitcast.127), calls=%async_computation | async-start | bytes 4194304 | tf_op jit(solution)/shard_map/all_to_all | solution.py:86
  41.3 1.3 collective-permute-start.1
  41.6 30.5 %copy-start.17 = (pred[2,2]{1,0:T(4,128)(4,1)}, pred[2,2]{1,0:T(4,128)(4,1)S(1)}, u32[]{:S(2)}) copy-start(pred[2,2]{1,0:T(4,128)(4,1)S(1)} %iota_compare_fusion.1) | copy-start | bytes 16
  70.7 2.7 collective-permute-start.2
  75.3 20.4 %all-to-all-start.1 = ((bf16[16,4,2048]{2,1,0:T(4,128)(2,1)}), bf16[16,4,2048]{2,1,0:T(4,128)(2,1)S(1)}, u32[]{:S(2)}, u32[]{:S(2)}) async-start(bf16[16,4,2048]{2,1,0:T(4,128)(2,1)} %reshape.246), calls=%async_computation.1 | async-start | bytes 524288 | tf_op jit(solution)/shard_map/all_to_all | solution.py:121
  95.7 33.3 %all-to-all-start.3 = ((bf16[16,8,2048]{2,1,0:T(8,128)(2,1)}), bf16[16,8,2048]{2,1,0:T(8,128)(2,1)}, u32[]{:S(2)}, u32[]{:S(2)}) async-start(bf16[16,8,2048]{2,1,0:T(8,128)(2,1)} %fusion.31), calls=%async_computation.4 | async-start | bytes 1048576 | tf_op jit(solution)/shard_map/all_to_all | solution.py:121
  106.2 58.7 %all-gather.4.cloned.1.call-start = ((), (), s32[]{:S(2)}) async-start(), calls=%async_computation.10 | async-start | bytes 1310720 | tf_op jit(solution)/shard_map/all_gather | solution.py:125
  107.1 70.8 %all-gather.6.cloned.1.call-start = ((), (), s32[]{:S(2)}) async-start(), calls=%async_computation.12 | async-start | bytes 2621440 | tf_op jit(solution)/shard_map/all_gather | solution.py:125
  129.1 87.6 %all-gather.8.cloned.1.call-start = ((), (), s32[]{:S(2)}) async-start(), calls=%async_computation.14 | async-start | bytes 2621440 | tf_op jit(solution)/shard_map/all_gather | solution.py:125
  164.8 82.9 %reduce-scatter.4.cloned.1.call-start = ((), (), s32[]{:S(2)}) async-start(), calls=%async_computation.11 | async-start | bytes 1310720 | tf_op jit(solution)/shard_map/reduce_scatter | solution.py:132
  174.7 112.3 %reduce-scatter.6.cloned.1.call-start = ((), (), s32[]{:S(2)}) async-start(), calls=%async_computation.13 | async-start | bytes 2621440 | tf_op jit(solution)/shard_map/reduce_scatter | solution.py:132
  191.7 133.4 %reduce-scatter.8.cloned.1.call-start = ((), (), s32[]{:S(2)}) async-start(), calls=%async_computation.15 | async-start | bytes 2621440 | tf_op jit(solution)/shard_map/reduce_scatter | solution.py:132
  273.3 63.9 %copy-start.11 = (pred[16,2,2,128]{3,2,1,0:T(4,128)(4,1)S(1)}, pred[16,2,2,128]{3,2,1,0:T(4,128)(4,1)}, u32[]{:S(2)}) copy-start(pred[16,2,2,128]{3,2,1,0:T(4,128)(4,1)} %copy-done.10) | copy-start | bytes 24580
  273.3 63.9 %copy-start.18 = (pred[2,2]{1,0:T(4,128)(4,1)S(1)}, pred[2,2]{1,0:T(4,128)(4,1)}, u32[]{:S(2)}) copy-start(pred[2,2]{1,0:T(4,128)(4,1)} %copy-done.17) | copy-start | bytes 16
  325.0 35.0 %all-to-all-start.6 = ((bf16[16,8,2048]{2,1,0:T(8,128)(2,1)}), bf16[16,8,2048]{2,1,0:T(8,128)(2,1)}, u32[]{:S(2)}, u32[]{:S(2)}) async-start(bf16[16,8,2048]{2,1,0:T(8,128)(2,1)} %bitcast.129), calls=%async_computation.9 | async-start | bytes 1048576 | tf_op jit(solution)/shard_map/all_to_all | solution.py:136
  338.9 4.4 %copy-start.8 = (bf16[16,2,4,2,128]{4,3,2,1,0:T(2,128)(2,1)S(1)}, bf16[16,2,4,2,128]{4,3,2,1,0:T(2,128)(2,1)}, u32[]{:S(2)}) copy-start(bf16[16,2,4,2,128]{4,3,2,1,0:T(2,128)(2,1)} %get-tuple-element.21) | copy-start | bytes 196612
  365.7 9.6 %copy-start.7 = (bf16[128,2048]{1,0:T(8,128)(2,1)S(1)}, bf16[128,2048]{1,0:T(8,128)(2,1)}, u32[]{:S(2)}) copy-start(bf16[128,2048]{1,0:T(8,128)(2,1)} %copy-done.5) | copy-start | bytes 1572868
  365.8 10.1 %copy-start.15 = (f32[2048]{0:T(1024)S(1)}, f32[2048]{0:T(1024)}, u32[]{:S(2)}) copy-start(f32[2048]{0:T(1024)} %param.31) | copy-start | bytes 24580
  365.8 10.1 %copy-start.16 = (f32[2048]{0:T(1024)S(1)}, f32[2048]{0:T(1024)}, u32[]{:S(2)}) copy-start(f32[2048]{0:T(1024)} %param.30) | copy-start | bytes 24580
  365.8 9.4 %collective-permute-start.3 = (f32[128,2048]{1,0:T(8,128)S(1)}, f32[128,2048]{1,0:T(8,128)S(1)}, u32[]{:S(2)}, u32[]{:S(2)}) collective-permute-start(f32[128,2048]{1,0:T(8,128)S(1)} %slice.71), channel_id=1, source_target_pairs={{0,4},{4,0},{1,5},{5,1},{2,6},{6,2},{3,7},{7,3},{8,12},{12,8},{9,1... | collective-permute-start | bytes 3145736 | tf_op jit(solution)/shard_map/ppermute | solution.py:21
  (13 other events, 31.6 us)
Sparse Core Ops, SparseCore 0:
  108.8 27.9 all-gather.3
  138.7 39.1 all-gather.5
  179.7 36.8 all-gather.7
  219.1 28.5 reduce-scatter.3
  250.1 36.8 reduce-scatter.5
  289.4 35.5 reduce-scatter.7
where the time goes:
time: 385 us; the launch traced here: 384 us
  waiting for transfers between devices  152 us (39%)
  blocking collectives  95.1 us (25%)
  matrix products  57.3 us (15%)
  starting transfers between devices  48.7 us (13%)
  between operations  13.9 us (4%)
  other arithmetic  11.9 us (3%)
  local copies, waits for them, and re-layouts  5.08 us (1%)
    all_to_all x2, blocking collectives, shards(): back = lax.all_to_all(ready, 'sp_0', 0, 0, tiled=True).reshape(-1, width)  59.5 us
    dot_general x17, matrix products, dot(): return jnp.dot(a, b, preferred_element_type=jnp.float32)  57.3 us
    all_to_all x1, blocking collectives, shards(): moved = lax.all_to_all(packed[i], 'sp_0', 0, 0, tiled=True)  35.6 us
    reduce_scatter x3, waiting for transfers between devices, shards(): lax.psum_scatter(piece, 'tp', scatter_dimension=0, tiled=True)  34 us
    all_to_all x2, waiting for transfers between devices, shards(): moved = lax.all_to_all(packed[i], 'sp_0', 0, 0, tiled=True)  30.3 us
    all_gather x3, waiting for transfers between devices, shards(): lax.all_gather(moved.reshape(-1, width), 'tp', axis=0, tiled=True)  27.9 us
    all_to_all x1, waiting for transfers between devices, shards(): lax.all_to_all(partial.reshape(n_tp, row_count // n_tp, width), 'tp', 0,...  24.7 us
    all_to_all x2, starting transfers between devices, shards(): moved = lax.all_to_all(packed[i], 'sp_0', 0, 0, tiled=True)  17 us
  transfers between devices with their start and end apart: 14, of which 13 were waited for; matrix products, arithmetic and copies ran while one was open for 14% of the time, Pallas kernels for 0%

commit v1 on v0

--- a/solution.py
+++ b/solution.py
@@ -10,6 +10,11 @@
 SUBLANES = 8
 residual_scale = 2.0**0.5
 norm_eps = 1e-05
+
+
+def tiled_gather(array, axis, dim):
+    copies = jnp.concatenate([array] * lax.axis_size(axis), axis=dim)
+    return lax.all_to_all(copies, axis, dim, dim, tiled=True)
 
 
 def next_in_sequence(x):
@@ -122,7 +127,7 @@
         rest = tuple(packed[i + 1 :])
         moved, rest = lax.optimization_barrier((moved, rest))
         packed[i + 1 :] = list(rest)
-        gathered.append(lax.all_gather(moved.reshape(-1, width), "tp", axis=0, tiled=True))
+        gathered.append(tiled_gather(moved.reshape(-1, width), "tp", 0))
     scattered = []
     for rows_in in gathered:
         gate_act = dot(rows_in, w_gate[0])

time: 385 us -> 394 us (1.023)
  starting transfers between devices: 48.7 us -> 94.1 us
  blocking collectives: 95.1 us -> 71.2 us
  waiting for transfers between devices: 152 us -> 131 us
  other arithmetic: 11.9 us -> 18.2 us
    reduce_scatter x3, waiting for transfers between devices: 34 us -> 0.04 us  [shards(): lax.psum_scatter(piece, 'tp', scatter_dimension=0, tiled=True)]
    all_gather x3 -> x0, waiting for transfers between devices: 27.9 us -> none  [shards(): lax.all_gather(moved.reshape(-1, width), 'tp', axis=0, tiled=True)]
    all_to_all x2 -> x1, blocking collectives: 59.5 us -> 32.3 us  [shards(): back = lax.all_to_all(ready, 'sp_0', 0, 0, tiled=True).reshape(-1, width)]
    all_to_all x2 -> x3, starting transfers between devices: 17 us -> 41.6 us  [shards(): moved = lax.all_to_all(packed[i], 'sp_0', 0, 0, tiled=True)]
    all_to_all x1 -> x2, waiting for transfers between devices: 14.9 us -> 35.8 us  [shards(): back = lax.all_to_all(ready, 'sp_0', 0, 0, tiled=True).reshape(-1, width)]
    all_to_all x0 -> x2, waiting for transfers between devices: none -> 14.7 us  [tiled_gather(): return lax.all_to_all(copies, axis, dim, dim, tiled=True)]
    all_to_all x1 -> x2, starting transfers between devices: 12.1 us -> 24.2 us  [shards(): back = lax.all_to_all(ready, 'sp_0', 0, 0, tiled=True).reshape(-1, width)]
    all_to_all x0 -> x2, starting transfers between devices: none -> 8.88 us  [tiled_gather(): return lax.all_to_all(copies, axis, dim, dim, tiled=True)]
  transfers between devices with their start and end apart: 14 -> 15, of which waited for: 13 -> 12; matrix products, arithmetic and copies ran while one was open for 14% -> 15% of each run, Pallas kernels for 0% -> 0%
where the time goes in v1:
time: 394 us; the launch traced here: 393 us
  waiting for transfers between devices  131 us (33%)
  starting transfers between devices  94.1 us (24%)
  blocking collectives  71.2 us (18%)
  matrix products  56.8 us (14%)
  other arithmetic  18.2 us (5%)
  between operations  13.6 us (3%)
  local copies, waits for them, and re-layouts  7.36 us (2%)
    dot_general x17, matrix products, dot(): return jnp.dot(a, b, preferred_element_type=jnp.float32)  56.8 us
    all_to_all x3, starting transfers between devices, shards(): moved = lax.all_to_all(packed[i], 'sp_0', 0, 0, tiled=True)  41.6 us
    all_to_all x1, blocking collectives, tiled_gather(): return lax.all_to_all(copies, axis, dim, dim, tiled=True)  39 us
    all_to_all x3, waiting for transfers between devices, shards(): moved = lax.all_to_all(packed[i], 'sp_0', 0, 0, tiled=True)  36.3 us
    all_to_all x2, waiting for transfers between devices, shards(): back = lax.all_to_all(ready, 'sp_0', 0, 0, tiled=True).reshape(-1, width)  35.8 us
    all_to_all x1, blocking collectives, shards(): back = lax.all_to_all(ready, 'sp_0', 0, 0, tiled=True).reshape(-1, width)  32.3 us
    all_to_all x1, waiting for transfers between devices, shards(): lax.all_to_all(partial.reshape(n_tp, row_count // n_tp, width), 'tp', 0,...  24.7 us
    all_to_all x2, starting transfers between devices, shards(): back = lax.all_to_all(ready, 'sp_0', 0, 0, tiled=True).reshape(-1, width)  24.2 us
  transfers between devices with their start and end apart: 15, of which 12 were waited for; matrix products, arithmetic and copies ran while one was open for 15% of the time, Pallas kernels for 0%

profile of v1, /device:TPU:33, one launch (start us, length us, event | category | flops | bytes accessed | tf_op | source)
XLA Modules:
  0.0 392.7 jit_solution(10408820525371587345)
XLA Ops:
  8.9 5.7 %collective-permute-start = (f32[4,384]{1,0:T(4,128)S(1)}, f32[4,384]{1,0:T(4,128)S(1)}, u32[]{:S(2)}, u32[]{:S(2)}) collective-permute-start(f32[4,384]{1,0:T(4,128)S(1)} %pad_maximum_fusion.8), channel_id=1, source_target_pairs={{0,4},{4,8},{8,12},{12,16},{16,20},{20,24},{24,28},{28,32},{32,36}... | collective-permute-start | bytes 18440 | tf_op jit(solution)/shard_map/ppermute | solution.py:22
  15.3 15.9 %collective-permute-done = f32[4,384]{1,0:T(4,128)S(1)} collective-permute-done((f32[4,384]{1,0:T(4,128)S(1)}, f32[4,384]{1,0:T(4,128)S(1)}, u32[]{:S(2)}, u32[]{:S(2)}) %collective-permute-start) | collective-permute-done | bytes 6176 | tf_op jit(solution)/shard_map/ppermute | solution.py:22
  36.6 4.7 %all-to-all-start = ((bf16[4,128,2048]{2,1,0:T(8,128)(2,1)}), bf16[4,128,2048]{2,1,0:T(8,128)(2,1)}, u32[]{:S(2)}, u32[]{:S(2)}) async-start(bf16[4,128,2048]{2,1,0:T(8,128)(2,1)} %bitcast.136), calls=%async_computation | async-start | bytes 4194304 | tf_op jit(solution)/shard_map/all_to_all | solution.py:91
  42.8 24.7 %all-to-all-done = bf16[4,128,2048]{2,1,0:T(8,128)(2,1)} async-done(((bf16[4,128,2048]{2,1,0:T(8,128)(2,1)}), bf16[4,128,2048]{2,1,0:T(8,128)(2,1)}, u32[]{:S(2)}, u32[]{:S(2)}) %all-to-all-start) | async-done | bytes 2097184 | tf_op jit(solution)/shard_map/all_to_all | solution.py:91
  75.3 6.6 %all-to-all-start.1 = ((bf16[16,4,2048]{2,1,0:T(4,128)(2,1)}), bf16[16,4,2048]{2,1,0:T(4,128)(2,1)S(1)}, u32[]{:S(2)}, u32[]{:S(2)}) async-start(bf16[16,4,2048]{2,1,0:T(4,128)(2,1)} %reshape.252), calls=%async_computation.1 | async-start | bytes 524288 | tf_op jit(solution)/shard_map/all_to_all | solution.py:126
  87.2 8.4 %all-to-all-done.1 = bf16[16,4,2048]{2,1,0:T(4,128)(2,1)S(1)} async-done(((bf16[16,4,2048]{2,1,0:T(4,128)(2,1)}), bf16[16,4,2048]{2,1,0:T(4,128)(2,1)S(1)}, u32[]{:S(2)}, u32[]{:S(2)}) %all-to-all-start.1) | async-done | bytes 262176 | tf_op jit(solution)/shard_map/all_to_all | solution.py:126
  96.4 10.4 %all-to-all-start.4 = ((bf16[16,8,2048]{2,1,0:T(8,128)(2,1)}), bf16[16,8,2048]{2,1,0:T(8,128)(2,1)}, u32[]{:S(2)}, u32[]{:S(2)}) async-start(bf16[16,8,2048]{2,1,0:T(8,128)(2,1)} %fusion.31), calls=%async_computation.5 | async-start | bytes 1048576 | tf_op jit(solution)/shard_map/all_to_all | solution.py:126
  108.9 20.7 %all-to-all-done.4 = bf16[16,8,2048]{2,1,0:T(8,128)(2,1)} async-done(((bf16[16,8,2048]{2,1,0:T(8,128)(2,1)}), bf16[16,8,2048]{2,1,0:T(8,128)(2,1)}, u32[]{:S(2)}, u32[]{:S(2)}) %all-to-all-start.4) | async-done | bytes 524320 | tf_op jit(solution)/shard_map/all_to_all | solution.py:126
  137.3 6.5 %all-to-all-done.2 = bf16[4,64,2048]{2,1,0:T(8,128)(2,1)} async-done(((bf16[4,64,2048]{2,1,0:T(8,128)(2,1)}), bf16[4,64,2048]{2,1,0:T(8,128)(2,1)}, u32[]{:S(2)}, u32[]{:S(2)}) %all-to-all-start.2) | async-done | bytes 1048608 | tf_op jit(solution)/shard_map/all_to_all | solution.py:17
  143.8 4.5 %all-to-all-start.5 = ((bf16[4,128,2048]{2,1,0:T(8,128)(2,1)}), bf16[4,128,2048]{2,1,0:T(8,128)(2,1)}, u32[]{:S(2)}, u32[]{:S(2)}) async-start(bf16[4,128,2048]{2,1,0:T(8,128)(2,1)} %bitcast.133), calls=%async_computation.6 | async-start | bytes 4194304 | tf_op jit(solution)/shard_map/all_to_all | solution.py:17
  152.5 5.5 %fusion.28 = bf16[256,2048]{1,0:T(8,128)(2,1)} fusion(bf16[1,768,2048]{2,1,0:T(8,128)(2,1)S(1)} %copy-done, bf16[256,2048]{1,0:T(8,128)(2,1)} %bitcast.11, bf16[1,2048,768]{2,1,0:T(8,128)(2,1)} %param.28, f32[256,768]{1,0:T(8,128)} %fusion.16), kind=kOutput, calls=%fused_computation.27 | convolution fusion | flops 1612316672 | bytes 9175040 | tf_op jit(solution)/shard_map/dot_general | solution.py:36
  158.1 8.2 %all-to-all-done.5 = bf16[4,128,2048]{2,1,0:T(8,128)(2,1)} async-done(((bf16[4,128,2048]{2,1,0:T(8,128)(2,1)}), bf16[4,128,2048]{2,1,0:T(8,128)(2,1)}, u32[]{:S(2)}, u32[]{:S(2)}) %all-to-all-start.5) | async-done | bytes 2097184 | tf_op jit(solution)/shard_map/all_to_all | solution.py:17
  166.3 24.6 %all-to-all-start.7 = ((bf16[16,8,2048]{2,1,0:T(8,128)(2,1)}), bf16[16,8,2048]{2,1,0:T(8,128)(2,1)}, u32[]{:S(2)}, u32[]{:S(2)}) async-start(bf16[16,8,2048]{2,1,0:T(8,128)(2,1)} %fusion.32), calls=%async_computation.9 | async-start | bytes 1048576 | tf_op jit(solution)/shard_map/all_to_all | solution.py:126
  191.2 5.6 %fusion.14 = f32[512,768]{1,0:T(8,128)} fusion(bf16[512,2048]{1,0:T(8,128)(2,1)} %bitcast.17, bf16[1,2048,768]{2,1,0:T(8,128)(2,1)} %param.27), kind=kOutput, calls=%fused_computation.15 | convolution fusion | flops 1610612736 | bytes 6815744 | tf_op jit(solution)/shard_map/dot_general | solution.py:36
  196.7 8.3 %fusion.18 = bf16[512,2048]{1,0:T(8,128)(2,1)} fusion(bf16[1,768,2048]{2,1,0:T(8,128)(2,1)S(1)} %copy-done, f32[512,768]{1,0:T(8,128)} %fusion.14, bf16[512,2048]{1,0:T(8,128)(2,1)} %bitcast.17, bf16[1,2048,768]{2,1,0:T(8,128)(2,1)} %param.28), kind=kOutput, calls=%fused_computation.19 | convolution fusion | flops 3224633344 | bytes 12058624 | tf_op jit(solution)/shard_map/dot_general | solution.py:36
  205.1 7.2 %all-to-all-done.7 = bf16[16,8,2048]{2,1,0:T(8,128)(2,1)} async-done(((bf16[16,8,2048]{2,1,0:T(8,128)(2,1)}), bf16[16,8,2048]{2,1,0:T(8,128)(2,1)}, u32[]{:S(2)}, u32[]{:S(2)}) %all-to-all-start.7) | async-done | bytes 524320 | tf_op jit(solution)/shard_map/all_to_all | solution.py:126
  214.3 39.0 %all_to_all.71 = bf16[4,128,2048]{2,1,0:T(8,128)(2,1)S(1)} all-to-all(bf16[4,128,2048]{2,1,0:T(8,128)(2,1)S(1)} %bitcast.134), channel_id=1, replica_groups=mesh['grp'=2,'sp_0'=16,'sp_1'=2,'tp'=4] {'tp'}, dimensions={0} | all-to-all | bytes 4194304 | tf_op jit(solution)/shard_map/all_to_all | solution.py:17
  257.6 8.3 %fusion.21 = bf16[512,2048]{1,0:T(8,128)(2,1)} fusion(bf16[1,768,2048]{2,1,0:T(8,128)(2,1)S(1)} %copy-done, f32[512,768]{1,0:T(8,128)} %fusion.12, bf16[512,2048]{1,0:T(8,128)(2,1)} %bitcast.138, bf16[1,2048,768]{2,1,0:T(8,128)(2,1)} %param.28), kind=kOutput, calls=%fused_computation.20 | convolution fusion | flops 3224633344 | bytes 12058624 | tf_op jit(solution)/shard_map/dot_general | solution.py:36
  267.0 32.3 %all_to_all.72 = bf16[16,4,2048]{2,1,0:T(4,128)(2,1)} all-to-all(bf16[16,4,2048]{2,1,0:T(4,128)(2,1)S(1)} %reshape.256), channel_id=1, replica_groups=mesh['grp'=2,'sp_0'=16,'sp_1'=2,'tp'=4] {'sp_0'}, dimensions={0} | all-to-all | bytes 524288 | tf_op jit(solution)/shard_map/all_to_all | solution.py:141
  299.2 11.7 %all-to-all-start.6 = ((bf16[16,8,2048]{2,1,0:T(8,128)(2,1)}), bf16[16,8,2048]{2,1,0:T(8,128)(2,1)}, u32[]{:S(2)}, u32[]{:S(2)}) async-start(bf16[16,8,2048]{2,1,0:T(8,128)(2,1)} %bitcast.139), calls=%async_computation.8 | async-start | bytes 1048576 | tf_op jit(solution)/shard_map/all_to_all | solution.py:141
  311.0 22.9 %all-to-all-done.6 = bf16[16,8,2048]{2,1,0:T(8,128)(2,1)} async-done(((bf16[16,8,2048]{2,1,0:T(8,128)(2,1)}), bf16[16,8,2048]{2,1,0:T(8,128)(2,1)}, u32[]{:S(2)}, u32[]{:S(2)}) %all-to-all-start.6) | async-done | bytes 524320 | tf_op jit(solution)/shard_map/all_to_all | solution.py:141
  333.9 12.5 %all-to-all-start.9 = ((bf16[16,8,2048]{2,1,0:T(8,128)(2,1)}), bf16[16,8,2048]{2,1,0:T(8,128)(2,1)}, u32[]{:S(2)}, u32[]{:S(2)}) async-start(bf16[16,8,2048]{2,1,0:T(8,128)(2,1)} %bitcast.140), calls=%async_computation.12 | async-start | bytes 1048576 | tf_op jit(solution)/shard_map/all_to_all | solution.py:141
  356.4 12.9 %all-to-all-done.9 = bf16[16,8,2048]{2,1,0:T(8,128)(2,1)} async-done(((bf16[16,8,2048]{2,1,0:T(8,128)(2,1)}), bf16[16,8,2048]{2,1,0:T(8,128)(2,1)}, u32[]{:S(2)}, u32[]{:S(2)}) %all-to-all-start.9) | async-done | bytes 524320 | tf_op jit(solution)/shard_map/all_to_all | solution.py:141
  375.1 7.2 %collective-permute-start.3 = (f32[128,2048]{1,0:T(8,128)S(1)}, f32[128,2048]{1,0:T(8,128)S(1)}, u32[]{:S(2)}, u32[]{:S(2)}) collective-permute-start(f32[128,2048]{1,0:T(8,128)S(1)} %slice.71), channel_id=1, source_target_pairs={{0,4},{4,0},{1,5},{5,1},{2,6},{6,2},{3,7},{7,3},{8,12},{12,8},{9,1... | collective-permute-start | bytes 3145736 | tf_op jit(solution)/shard_map/ppermute | solution.py:26
  (125 shorter events, 65.0 us)
Async XLA Ops:
  6.5 145.9 %copy-start = (bf16[1,768,2048]{2,1,0:T(8,128)(2,1)S(1)}, bf16[1,768,2048]{2,1,0:T(8,128)(2,1)}, u32[]{:S(2)}) copy-start(bf16[1,768,2048]{2,1,0:T(8,128)(2,1)} %param.29) | copy-start | bytes 9437188
  8.9 22.4 %collective-permute-start = (f32[4,384]{1,0:T(4,128)S(1)}, f32[4,384]{1,0:T(4,128)S(1)}, u32[]{:S(2)}, u32[]{:S(2)}) collective-permute-start(f32[4,384]{1,0:T(4,128)S(1)} %pad_maximum_fusion.8), channel_id=1, source_target_pairs={{0,4},{4,8},{8,12},{12,16},{16,20},{20,24},{24,28},{28,32},{32,36}... | collective-permute-start | bytes 18440 | tf_op jit(solution)/shard_map/ppermute | solution.py:22
  36.6 30.9 %all-to-all-start = ((bf16[4,128,2048]{2,1,0:T(8,128)(2,1)}), bf16[4,128,2048]{2,1,0:T(8,128)(2,1)}, u32[]{:S(2)}, u32[]{:S(2)}) async-start(bf16[4,128,2048]{2,1,0:T(8,128)(2,1)} %bitcast.136), calls=%async_computation | async-start | bytes 4194304 | tf_op jit(solution)/shard_map/all_to_all | solution.py:91
  41.3 1.3 collective-permute-start.1
  41.6 30.5 %copy-start.18 = (pred[2,2]{1,0:T(4,128)(4,1)}, pred[2,2]{1,0:T(4,128)(4,1)S(1)}, u32[]{:S(2)}) copy-start(pred[2,2]{1,0:T(4,128)(4,1)S(1)} %iota_compare_fusion.1) | copy-start | bytes 16
  70.7 2.7 collective-permute-start.2
  75.3 20.4 %all-to-all-start.1 = ((bf16[16,4,2048]{2,1,0:T(4,128)(2,1)}), bf16[16,4,2048]{2,1,0:T(4,128)(2,1)S(1)}, u32[]{:S(2)}, u32[]{:S(2)}) async-start(bf16[16,4,2048]{2,1,0:T(4,128)(2,1)} %reshape.252), calls=%async_computation.1 | async-start | bytes 524288 | tf_op jit(solution)/shard_map/all_to_all | solution.py:126
  96.4 33.3 %all-to-all-start.4 = ((bf16[16,8,2048]{2,1,0:T(8,128)(2,1)}), bf16[16,8,2048]{2,1,0:T(8,128)(2,1)}, u32[]{:S(2)}, u32[]{:S(2)}) async-start(bf16[16,8,2048]{2,1,0:T(8,128)(2,1)} %fusion.31), calls=%async_computation.5 | async-start | bytes 1048576 | tf_op jit(solution)/shard_map/all_to_all | solution.py:126
  129.7 14.1 %all-to-all-start.2 = ((bf16[4,64,2048]{2,1,0:T(8,128)(2,1)}), bf16[4,64,2048]{2,1,0:T(8,128)(2,1)}, u32[]{:S(2)}, u32[]{:S(2)}) async-start(bf16[4,64,2048]{2,1,0:T(8,128)(2,1)} %bitcast.135), calls=%async_computation.2 | async-start | bytes 2097152 | tf_op jit(solution)/shard_map/all_to_all | solution.py:17
  143.8 22.5 %all-to-all-start.5 = ((bf16[4,128,2048]{2,1,0:T(8,128)(2,1)}), bf16[4,128,2048]{2,1,0:T(8,128)(2,1)}, u32[]{:S(2)}, u32[]{:S(2)}) async-start(bf16[4,128,2048]{2,1,0:T(8,128)(2,1)} %bitcast.133), calls=%async_computation.6 | async-start | bytes 4194304 | tf_op jit(solution)/shard_map/all_to_all | solution.py:17
  148.3 117.6 %reduce-scatter.4.cloned.1.call-start = ((), (), s32[]{:S(2)}) async-start(), calls=%async_computation.13 | async-start | bytes 1310720 | tf_op jit(solution)/shard_map/reduce_scatter | solution.py:137
  166.3 46.0 %all-to-all-start.7 = ((bf16[16,8,2048]{2,1,0:T(8,128)(2,1)}), bf16[16,8,2048]{2,1,0:T(8,128)(2,1)}, u32[]{:S(2)}, u32[]{:S(2)}) async-start(bf16[16,8,2048]{2,1,0:T(8,128)(2,1)} %fusion.32), calls=%async_computation.9 | async-start | bytes 1048576 | tf_op jit(solution)/shard_map/all_to_all | solution.py:126
  190.9 108.3 %reduce-scatter.6.cloned.1.call-start = ((), (), s32[]{:S(2)}) async-start(), calls=%async_computation.14 | async-start | bytes 2621440 | tf_op jit(solution)/shard_map/reduce_scatter | solution.py:137
  205.1 105.9 %reduce-scatter.8.cloned.1.call-start = ((), (), s32[]{:S(2)}) async-start(), calls=%async_computation.15 | async-start | bytes 2621440 | tf_op jit(solution)/shard_map/reduce_scatter | solution.py:137
  214.3 40.3 %copy-start.22 = (bf16[1,2048,768]{2,1,0:T(8,128)(2,1)S(1)}, bf16[1,2048,768]{2,1,0:T(8,128)(2,1)}, u32[]{:S(2)}) copy-start(bf16[1,2048,768]{2,1,0:T(8,128)(2,1)} %param.27) | copy-start | bytes 9437188
  299.2 47.2 %copy-start.12 = (pred[16,2,2,128]{3,2,1,0:T(4,128)(4,1)S(1)}, pred[16,2,2,128]{3,2,1,0:T(4,128)(4,1)}, u32[]{:S(2)}) copy-start(pred[16,2,2,128]{3,2,1,0:T(4,128)(4,1)} %copy-done.11) | copy-start | bytes 24580
  299.2 47.2 %copy-start.19 = (pred[2,2]{1,0:T(4,128)(4,1)S(1)}, pred[2,2]{1,0:T(4,128)(4,1)}, u32[]{:S(2)}) copy-start(pred[2,2]{1,0:T(4,128)(4,1)} %copy-done.18) | copy-start | bytes 16
  299.2 34.6 %all-to-all-start.6 = ((bf16[16,8,2048]{2,1,0:T(8,128)(2,1)}), bf16[16,8,2048]{2,1,0:T(8,128)(2,1)}, u32[]{:S(2)}, u32[]{:S(2)}) async-start(bf16[16,8,2048]{2,1,0:T(8,128)(2,1)} %bitcast.139), calls=%async_computation.8 | async-start | bytes 1048576 | tf_op jit(solution)/shard_map/all_to_all | solution.py:141
  333.9 35.4 %all-to-all-start.9 = ((bf16[16,8,2048]{2,1,0:T(8,128)(2,1)}), bf16[16,8,2048]{2,1,0:T(8,128)(2,1)}, u32[]{:S(2)}, u32[]{:S(2)}) async-start(bf16[16,8,2048]{2,1,0:T(8,128)(2,1)} %bitcast.140), calls=%async_computation.12 | async-start | bytes 1048576 | tf_op jit(solution)/shard_map/all_to_all | solution.py:141
  348.2 5.4 %copy-start.9 = (bf16[16,2,4,2,128]{4,3,2,1,0:T(2,128)(2,1)S(1)}, bf16[16,2,4,2,128]{4,3,2,1,0:T(2,128)(2,1)}, u32[]{:S(2)}) copy-start(bf16[16,2,4,2,128]{4,3,2,1,0:T(2,128)(2,1)} %get-tuple-element.21) | copy-start | bytes 196612
  375.0 9.6 %copy-start.7 = (bf16[128,2048]{1,0:T(8,128)(2,1)S(1)}, bf16[128,2048]{1,0:T(8,128)(2,1)}, u32[]{:S(2)}) copy-start(bf16[128,2048]{1,0:T(8,128)(2,1)} %copy-done.5) | copy-start | bytes 1572868
  375.1 10.1 %copy-start.16 = (f32[2048]{0:T(1024)S(1)}, f32[2048]{0:T(1024)}, u32[]{:S(2)}) copy-start(f32[2048]{0:T(1024)} %param.31) | copy-start | bytes 24580
  375.1 10.1 %copy-start.17 = (f32[2048]{0:T(1024)S(1)}, f32[2048]{0:T(1024)}, u32[]{:S(2)}) copy-start(f32[2048]{0:T(1024)} %param.30) | copy-start | bytes 24580
  375.1 9.4 %collective-permute-start.3 = (f32[128,2048]{1,0:T(8,128)S(1)}, f32[128,2048]{1,0:T(8,128)S(1)}, u32[]{:S(2)}, u32[]{:S(2)}) collective-permute-start(f32[128,2048]{1,0:T(8,128)S(1)} %slice.71), channel_id=1, source_target_pairs={{0,4},{4,0},{1,5},{5,1},{2,6},{6,2},{3,7},{7,3},{8,12},{12,8},{9,1... | collective-permute-start | bytes 3145736 | tf_op jit(solution)/shard_map/ppermute | solution.py:26
  (16 other events, 40.4 us)
Sparse Core Ops, SparseCore 0:
  158.2 36.8 reduce-scatter.3
  205.2 55.6 reduce-scatter.5
  266.0 44.0 reduce-scatter.7
